TPU v7x, 32 devices: a whole 2x2x4 slice. The times are simulated.
32 devices in a mesh: ep: 8 (over z, y), tp: 4 (over x, core).
Axes of the slice: x: 2, y: 2, z: 4, core: 2. Of those that a mesh axis runs over, the one named last changes fastest.
Arguments:
- gate_outer: bfloat16 [16384, 1024], P(('ep', 'tp')), may hold values from -6 to 6
- gate_inner: bfloat16 [16384, 1024], P(('ep', 'tp')), may hold values from -6 to 6
- conv_input: bfloat16 [16384, 1024], P(('ep', 'tp')), may hold values from -6 to 6
- conv_taps: float32 [3, 1024], replicated, may hold values from -3.5 to 3.5
- mixer_out_weight: bfloat16 [1024, 2048], replicated, may hold values from -0.1875 to 0.1875
- moe_tokens: bfloat16 [4096, 2048], P(('ep', 'tp')), may hold values from -40 to 40
- norm_gain: float32 [2048], replicated, may hold values from 0.1 to 1.9
- expert_ids: int32 [4096, 4], P(('ep', 'tp')), may hold values from 0 to 31, all different within a row; in each aligned block of 128 rows (0 to 127, 128 to 255, ...) at most 24 rows name the same one
- route_weight: float32 [4096, 4], P(('ep', 'tp')), may hold values from 0.2 to 1
- expert_gate: bfloat16 [32, 2048, 1024], P(('ep', 'tp')), may hold values from -0.39648438 to 0.39648438
- expert_up: bfloat16 [32, 2048, 1024], P(('ep', 'tp')), may hold values from -0.39648438 to 0.39648438
- expert_down: bfloat16 [32, 1024, 2048], P(('ep', 'tp')), may hold values from -0.03125 to 0.03125
Outputs:
- mixed_out: bfloat16 [16384, 2048], P(('ep', 'tp'))
- moe_out: bfloat16 [4096, 2048], P(('ep', 'tp'))
Inputs may be any that keep to these rules, and one draw needn't show every extreme that they name: `expert_ids`: each token names 4 different experts. Among the tokens of one device no expert is named by more than 24 of them, and on some device an expert is named by exactly 24.
All inputs are finite; a program needn't handle non-finite values.
Results may differ from a plain program's by a relative error of at most 0.007.
Values may be sent and summed in bfloat16 or wider, within the bound.
No kernel may reach another device: no remote copies, remote signals or barrier semaphores. Data moves between devices by JAX's collectives and lax.ppermute only.
A program may use at most 128 MiB of HBM per device.

v0:
```python
import functools
import math

import jax
import jax.numpy as jnp
from jax import lax
from jax.experimental import pallas as pl
from jax.experimental.pallas import tpu as pltpu
from jax.sharding import Mesh, PartitionSpec as P

epsilon = 1e-06
clamp_limit = 7.0
alpha_gate = 1.702
EVERY = ("half", "near", "tp")
NEAR = ("near", "tp")
SMALL_VMEM = 12 * 1024 * 1024
WIDE_VMEM = 58 * 1024 * 1024
EXPERT_VMEM = 50 * 1024 * 1024
AHEAD = 5


def from_behind(value, axis, by):
    length = lax.axis_size(axis)
    pairs = [(i, i + by) for i in range(length) if 0 <= i + by < length]
    return lax.ppermute(value, axis, pairs)


def swap_halves(value):
    halves, near = lax.axis_size("half"), lax.axis_size("near")
    shift = near // 2 if near % 2 == 0 and halves > 1 else 0
    pairs = [
        (h * near + n, (h + 1) % halves * near + (n + shift) % near)
        for h in range(halves)
        for n in range(near)
    ]
    return lax.ppermute(value, ("half", "near"), pairs)


def dispatch_kernel(capacity, masked, ids_ref, rows_ref, slot_ref, *send_refs):
    top_count, tokens = ids_ref.shape
    slots = sum(ref.shape[0] for ref in send_refs)
    experts_near = slots // capacity
    ids = ids_ref[...] - lax.axis_index("half") * experts_near
    member = lax.axis_index("near") * lax.axis_size("tp") + lax.axis_index("tp")
    experts = lax.broadcasted_iota(jnp.int32, (experts_near, tokens), 0)
    hits = [ids[k : k + 1, :] == experts for k in range(top_count)]
    named = functools.reduce(jnp.logical_or, hits)
    before = lax.broadcasted_iota(jnp.int32, (tokens, tokens), 0) < lax.broadcasted_iota(
        jnp.int32, (tokens, tokens), 1
    )
    rank = jnp.dot(
        named.astype(jnp.float32).astype(jnp.bfloat16),
        before.astype(jnp.float32).astype(jnp.bfloat16),
        preferred_element_type=jnp.float32,
    )
    slot_rows = lax.broadcasted_iota(jnp.int32, (slots, tokens), 0)
    here = None
    for k in range(top_count):
        own = jnp.sum(jnp.where(hits[k], rank, 0.0), axis=0, keepdims=True).astype(jnp.int32)
        choice = ids[k : k + 1, :]
        inside = (choice >= 0) & (choice < experts_near)
        block = choice ^ member if masked else choice
        slot = jnp.where(inside, block * capacity + own, slots)
        slot_ref[k : k + 1, :] = slot
        match = slot_rows == slot
        here = match if here is None else here | match
    laid = jnp.dot(
        here.astype(jnp.float32).astype(jnp.bfloat16),
        rows_ref[...],
        preferred_element_type=jnp.float32,
    )
    start = 0
    for ref in send_refs:
        ref[...] = laid[start : start + ref.shape[0]].astype(ref.dtype)
        start += ref.shape[0]


def block_shapes(slots, width, blocks):
    return [jax.ShapeDtypeStruct((slots // blocks, width), jnp.bfloat16)] * blocks


def to_slots(ids, rows, slots, capacity, blocks, room):
    top_count, tokens = ids.shape
    width = rows.shape[1]
    held = pl.BlockSpec(memory_space=pltpu.VMEM)
    slot, *send = pl.pallas_call(
        functools.partial(dispatch_kernel, capacity, blocks > 1),
        in_specs=[held, held],
        out_specs=[held] * (1 + blocks),
        out_shape=[jax.ShapeDtypeStruct((top_count, tokens), jnp.int32)]
        + block_shapes(slots, width, blocks),
        compiler_params=pltpu.CompilerParams(vmem_limit_bytes=room),
        cost_estimate=pl.CostEstimate(
            flops=2 * slots * tokens * width,
            bytes_accessed=2 * (slots + tokens) * width,
            transcendentals=0,
        ),
    )(ids, rows)
    return slot, send


def gather_blocks(refs, wide_ref):
    if len(refs) == 1:
        return refs[0][...]
    start = 0
    for ref in refs:
        wide_ref[start : start + ref.shape[0], :] = ref[...].astype(jnp.float32)
        start += ref.shape[0]
    return wide_ref[...].astype(jnp.bfloat16)


def combine_kernel(blocks, addends, slot_ref, weight_ref, *refs):
    back_refs, add_refs = refs[:blocks], refs[blocks : blocks + addends]
    out_ref, wide_ref = refs[blocks + addends :]
    slots = sum(ref.shape[0] for ref in back_refs)
    top_count, tokens = slot_ref.shape
    weights = weight_ref[...]
    mix = weights / jnp.sum(weights, axis=0, keepdims=True)
    slot_rows = lax.broadcasted_iota(jnp.int32, (slots, tokens), 0)
    share = jnp.zeros((slots, tokens), jnp.float32)
    for k in range(top_count):
        share = jnp.where(slot_rows == slot_ref[k : k + 1, :], mix[k : k + 1, :], share)
    high = share.astype(jnp.bfloat16)
    low = (share - high.astype(jnp.float32)).astype(jnp.bfloat16)
    back = gather_blocks(back_refs, wide_ref)
    over = (((0,), (0,)), ((), ()))
    total = lax.dot_general(high, back, over, preferred_element_type=jnp.float32)
    total = total + lax.dot_general(low, back, over, preferred_element_type=jnp.float32)
    for ref in add_refs:
        total = total + ref[...].astype(jnp.float32)
    out_ref[...] = total.astype(out_ref.dtype)


def from_slots(slot, weights, back, addends):
    slots, width = sum(block.shape[0] for block in back), back[0].shape[1]
    tokens = slot.shape[1]
    wide = (slots, width) if len(back) > 1 else (8, 128)
    return pl.pallas_call(
        functools.partial(combine_kernel, len(back), len(addends)),
        in_specs=[pl.BlockSpec(memory_space=pltpu.VMEM)] * (2 + len(back) + len(addends)),
        out_specs=pl.BlockSpec(memory_space=pltpu.VMEM),
        out_shape=jax.ShapeDtypeStruct((tokens, width), jnp.bfloat16),
        scratch_shapes=[pltpu.VMEM(wide, jnp.float32)],
        compiler_params=pltpu.CompilerParams(vmem_limit_bytes=SMALL_VMEM),
        cost_estimate=pl.CostEstimate(
            flops=4 * slots * tokens * width,
            bytes_accessed=2 * (slots + tokens) * width,
            transcendentals=0,
        ),
    )(slot, weights, *back, *addends)


def expert_kernel(blocks, gain, gate, up, down, *refs):
    in_refs, out_refs = refs[:blocks], refs[blocks : 2 * blocks]
    gate_ref, up_ref, down_ref, hidden_ref, wide_ref, rows_ref, gain_ref, sems = refs[2 * blocks :]
    parts, _, tile = gate_ref.shape
    columns, _, column = down_ref.shape
    work = []
    for part in range(parts):
        cut = pl.ds(part * tile, tile)
        work.append(((gate, gate_ref, part, cut), (up, up_ref, part, cut)))
    for part in range(columns):
        work.append(((down, down_ref, part, pl.ds(part * column, column)),))
    copies = [
        [
            pltpu.make_async_copy(source.at[0, :, cut], target.at[part], sems.at[step, at])
            for at, (source, target, part, cut) in enumerate(pieces)
        ]
        for step, pieces in enumerate(work)
    ]

    def ready(step):
        for copy in copies[step]:
            copy.wait()
        if step + AHEAD < len(copies):
            for copy in copies[step + AHEAD]:
                copy.start()

    scale_copy = pltpu.make_async_copy(gain, gain_ref, sems.at[len(copies), 0])
    scale_copy.start()
    for step in range(min(AHEAD, len(copies))):
        for copy in copies[step]:
            copy.start()
    height = in_refs[0].shape[0]
    for block, ref in enumerate(in_refs):
        wide_ref[block * height : (block + 1) * height, :] = ref[...].astype(jnp.float32)
    scale_copy.wait()
    count = wide_ref.shape[0]
    band = math.gcd(count, 64)
    for top in range(0, count, band):
        tokens = wide_ref[top : top + band, :]
        scale = lax.rsqrt(jnp.mean(tokens * tokens, axis=-1, keepdims=True) + epsilon)
        rows_ref[top : top + band, :] = (tokens * scale * gain_ref[...]).astype(jnp.bfloat16)
    for part in range(parts):
        ready(part)
        rows = rows_ref[...]
        gate_pre = jnp.dot(rows, gate_ref[part], preferred_element_type=jnp.float32)
        up_pre = jnp.dot(rows, up_ref[part], preferred_element_type=jnp.float32)
        gate_pre = jnp.minimum(gate_pre, clamp_limit)
        up_pre = jnp.clip(up_pre, -clamp_limit, clamp_limit)
        hidden_ref[:, part * tile : (part + 1) * tile] = (
            (up_pre + 1.0) * (gate_pre * jax.nn.sigmoid(alpha_gate * gate_pre))
        ).astype(jnp.bfloat16)
    for part in range(columns):
        ready(parts + part)
        result = jnp.dot(hidden_ref[...], down_ref[part], preferred_element_type=jnp.float32)
        start = 0
        for ref in out_refs:
            ref[:, part * column : (part + 1) * column] = result[
                start : start + ref.shape[0]
            ].astype(ref.dtype)
            start += ref.shape[0]


def expert_rows(rows, gain, weights, room):
    count, width = sum(block.shape[0] for block in rows), rows[0].shape[1]
    hidden = weights[0].shape[2]
    tile, column = math.gcd(hidden, 256), math.gcd(width, 512)
    parts, columns = hidden // tile, width // column
    held = pl.BlockSpec(memory_space=pltpu.VMEM)
    return pl.pallas_call(
        functools.partial(expert_kernel, len(rows)),
        in_specs=[pl.BlockSpec(memory_space=pl.ANY)] * 4 + [held] * len(rows),
        out_specs=[held] * len(rows),
        out_shape=block_shapes(count, width, len(rows)),
        scratch_shapes=[
            pltpu.VMEM((parts, width, tile), jnp.bfloat16),
            pltpu.VMEM((parts, width, tile), jnp.bfloat16),
            pltpu.VMEM((columns, hidden, column), jnp.bfloat16),
            pltpu.VMEM((count, hidden), jnp.bfloat16),
            pltpu.VMEM((count, width), jnp.float32),
            pltpu.VMEM((count, width), jnp.bfloat16),
            pltpu.VMEM(gain.shape, gain.dtype),
            pltpu.SemaphoreType.DMA((parts + columns + 1, 2)),
        ],
        compiler_params=pltpu.CompilerParams(vmem_limit_bytes=room),
        cost_estimate=pl.CostEstimate(
            flops=6 * count * width * hidden,
            bytes_accessed=2 * (3 * width * hidden + 2 * count * width),
            transcendentals=count * hidden,
        ),
    )(gain, *weights, *rows)


def hop_order(members):
    half = members // 2
    return [half | mask for mask in range(half)] + list(range(half - 1, 0, -1))


def hops(blocks, masks):
    members = len(blocks)
    arrived = {
        mask: lax.ppermute(blocks[mask], NEAR, [(i, i ^ mask) for i in range(members)])
        for mask in masks
    }
    return arrived


def in_order(first, arrived):
    return [first] + [arrived[mask] for mask in sorted(arrived)]


def exchange(rows, members):
    parts = rows.reshape(members, -1, rows.shape[1])
    return lax.all_to_all(parts, NEAR, split_axis=0, concat_axis=0, tiled=True).reshape(rows.shape)


def gated_input(gate_inner, conv_input):
    return (gate_inner.astype(jnp.float32) * conv_input.astype(jnp.float32)).astype(jnp.bfloat16)


def mixer(gate_outer, gate_inner, conv_input, previous, conv_taps, mixer_out_weight):
    rows_here = gate_inner.shape[0]
    product = gated_input(gate_inner, conv_input)
    extended = jnp.concatenate([previous, product], 0).astype(jnp.float32)
    convolved = jnp.zeros(product.shape, jnp.float32)
    for offset in range(conv_taps.shape[0]):
        convolved = convolved + conv_taps[offset][None, :] * extended[offset : offset + rows_here]
    gated_rows = (gate_outer.astype(jnp.float32) * convolved).astype(jnp.bfloat16)
    return jnp.dot(gated_rows, mixer_out_weight, preferred_element_type=jnp.float32).astype(
        jnp.bfloat16
    )


def shards(
    gate_outer,
    gate_inner,
    conv_input,
    conv_taps,
    mixer_out_weight,
    moe_tokens,
    norm_gain,
    expert_ids,
    route_weight,
    expert_gate,
    expert_up,
    expert_down,
):
    tokens_here, top_count = expert_ids.shape
    members = lax.axis_size(NEAR)
    capacity = 3 * tokens_here * top_count // (2 * lax.axis_size(EVERY))
    capacity = -(-capacity // 8) * 8
    slots = members * capacity
    masks = hop_order(members)
    gain = norm_gain[None, :]
    ids, route = expert_ids.T, route_weight.T
    weights = (expert_gate, expert_up, expert_down)

    far_tokens = swap_halves(moe_tokens)
    far_ids = swap_halves(ids)
    far_route = swap_halves(route)
    last = gate_inner.shape[0] - (conv_taps.shape[0] - 1)
    previous = from_behind(gated_input(gate_inner[last:], conv_input[last:]), EVERY, 1)
    slot, send = to_slots(ids, moe_tokens, slots, capacity, members, WIDE_VMEM)
    first_go, first_back = members * 7 // 16, members // 2
    received = hops(send, masks[:first_go])
    far_slot, far_send = to_slots(far_ids, far_tokens, slots, capacity, 1, SMALL_VMEM)
    far_received = exchange(far_send[0], members)
    received |= hops(send, masks[first_go:])
    received = in_order(send[0], received)
    far_out = expert_rows([far_received], gain, weights, EXPERT_VMEM)
    far_back = exchange(far_out[0], members)
    out = expert_rows(received, gain, weights, WIDE_VMEM)
    back = hops(out, masks[:first_back])
    far_total = from_slots(far_slot, far_route, [far_back], ())
    returned = swap_halves(far_total)
    back |= hops(out, masks[first_back:])
    mixed_out = mixer(
        gate_outer, gate_inner, conv_input, previous, conv_taps, mixer_out_weight
    )
    back = in_order(out[0], back)
    moe_out = from_slots(slot, route, back, (returned,))
    return (mixed_out, moe_out)


def solution(mesh):
    outer, inner = mesh.shape["ep"], mesh.shape["tp"]
    halves = 2 if outer % 2 == 0 else 1
    split = Mesh(mesh.devices.reshape(halves, outer // halves, inner), EVERY)
    rows = P(EVERY, None)
    weights = P(EVERY, None, None)
    in_specs = (rows, rows, rows, P(), P(), rows, P(), rows, rows, weights, weights, weights)
    return jax.shard_map(
        shards, mesh=split, in_specs=in_specs, out_specs=(rows, rows), check_vma=False
    )
```

profile of v0, /device:TPU:16, one launch (start us, length us, event | category | flops | bytes accessed | tf_op | source)
XLA Modules:
  0.0 176.6 jit_solution(11773743144501640122)
XLA Ops:
  2.7 23.2 %collective-permute-done.31.ids_ref = s32[4,128]{1,0:T(4,128)S(1)} collective-permute-done((s32[4,128]{1,0:T(4,128)}, s32[4,128]{1,0:T(4,128)S(1)}, u32[]{:S(2)}, u32[]{:S(2)}) %collective-permute-start.31) | collective-permute-done | bytes 2080 | tf_op jit(solution)/shard_map/ppermute | solution.py:36
  26.6 25.4 %all_to_all.10 = bf16[16,24,2048]{2,1,0:T(8,128)(2,1)S(1)} all-to-all(bf16[16,24,2048]{2,1,0:T(8,128)(2,1)S(1)} %bitcast.12), channel_id=1, replica_groups=mesh['half'=2,'near'=4,'tp'=4] {'near','tp'}, dimensions={0} | all-to-all | bytes 3145728 | tf_op jit(solution)/shard_map/all_to_all | solution.py:265
  52.0 9.2 %shard_map.134 = bf16[384,2048]{1,0:T(8,128)(2,1)} custom-call(f32[1,2048]{1,0:T(1,128)S(1)} %bitcast.17, bf16[1,2048,1024]{2,1,0:T(8,128)(2,1)} %gate.3, bf16[1,2048,1024]{2,1,0:T(8,128)(2,1)} %up.3, bf16[1,1024,2048]{2,1,0:T(8,128)(2,1)} %down.3, bf16[384,2048]{1,0:T(8,128)(2,1)S(1)} %bitcast.13), custom_call_target="tpu_custom_call" | custom-call | flops 4831838208 | bytes 15728640 | tf_op jit(solution)/shard_map/pallas_call | solution.py:221
  61.2 3.9 %all-to-all-start.1 = ((bf16[16,24,2048]{2,1,0:T(8,128)(2,1)}), bf16[16,24,2048]{2,1,0:T(8,128)(2,1)S(1)}, u32[]{:S(2)}, u32[]{:S(2)}) async-start(bf16[16,24,2048]{2,1,0:T(8,128)(2,1)} %bitcast.8), calls=%async_computation.1 | async-start | bytes 3145728 | tf_op jit(solution)/shard_map/all_to_all | solution.py:265
  65.1 2.8 %shard_map.131 = (s32[4,128]{1,0:T(4,128)}, bf16[24,2048]{1,0:T(8,128)(2,1)}, bf16[24,2048]{1,0:T(8,128)(2,1)}, bf16[24,2048]{1,0:T(8,128)(2,1)}, bf16[24,2048]{...) custom-call(s32[4,128]{1,0:T(4,128)} %bitcast.22, ...), custom_call_target="tpu_custom_call" | custom-call | flops 201326592 | bytes 2097152 | tf_op jit(solution)/shard_map/pallas_call | solution.py:86
  68.2 2.6 %collective-permute-start.10 = (bf16[24,2048]{1,0:T(8,128)(2,1)}, bf16[24,2048]{1,0:T(8,128)(2,1)S(1)}, u32[]{:S(2)}, u32[]{:S(2)}) collective-permute-start(bf16[24,2048]{1,0:T(8,128)(2,1)} %get-tuple-element.48), channel_id=1, source_target_pairs={{0,10},{1,11},{2,8},{3,9},{4,14},{5,15},{6,12},{7,13},{8,2},{9,3},... | collective-permute-start | bytes 294920 | tf_op jit(solution)/shard_map/ppermute | solution.py:253
  70.8 2.6 %collective-permute-start.12 = (bf16[24,2048]{1,0:T(8,128)(2,1)}, bf16[24,2048]{1,0:T(8,128)(2,1)S(1)}, u32[]{:S(2)}, u32[]{:S(2)}) collective-permute-start(bf16[24,2048]{1,0:T(8,128)(2,1)} %get-tuple-element.50), channel_id=1, source_target_pairs={{0,12},{1,13},{2,14},{3,15},{4,8},{5,9},{6,10},{7,11},{8,4},{9,5},... | collective-permute-start | bytes 294920 | tf_op jit(solution)/shard_map/ppermute | solution.py:253
  73.5 3.5 %collective-permute-start.14 = (bf16[24,2048]{1,0:T(8,128)(2,1)}, bf16[24,2048]{1,0:T(8,128)(2,1)S(1)}, u32[]{:S(2)}, u32[]{:S(2)}) collective-permute-start(bf16[24,2048]{1,0:T(8,128)(2,1)} %get-tuple-element.52), channel_id=1, source_target_pairs={{0,14},{1,15},{2,12},{3,13},{4,10},{5,11},{6,8},{7,9},{8,6},{9,7},... | collective-permute-start | bytes 294920 | tf_op jit(solution)/shard_map/ppermute | solution.py:253
  77.0 12.7 %collective-permute-done.10.refs_10_ = bf16[24,2048]{1,0:T(8,128)(2,1)S(1)} collective-permute-done((bf16[24,2048]{1,0:T(8,128)(2,1)}, bf16[24,2048]{1,0:T(8,128)(2,1)S(1)}, u32[]{:S(2)}, u32[]{:S(2)}) %collective-permute-start.10) | collective-permute-done | bytes 98336 | tf_op jit(solution)/shard_map/ppermute | solution.py:253
  90.7 3.3 %collective-permute-done.12.refs_12_ = bf16[24,2048]{1,0:T(8,128)(2,1)S(1)} collective-permute-done((bf16[24,2048]{1,0:T(8,128)(2,1)}, bf16[24,2048]{1,0:T(8,128)(2,1)S(1)}, u32[]{:S(2)}, u32[]{:S(2)}) %collective-permute-start.12) | collective-permute-done | bytes 98336 | tf_op jit(solution)/shard_map/ppermute | solution.py:253
  95.0 3.7 %collective-permute-done.14.refs_14_ = bf16[24,2048]{1,0:T(8,128)(2,1)S(1)} collective-permute-done((bf16[24,2048]{1,0:T(8,128)(2,1)}, bf16[24,2048]{1,0:T(8,128)(2,1)S(1)}, u32[]{:S(2)}, u32[]{:S(2)}) %collective-permute-start.14) | collective-permute-done | bytes 98336 | tf_op jit(solution)/shard_map/ppermute | solution.py:253
  100.8 1.7 collective-permute-start.7
  105.0 3.7 %collective-permute-done.5.refs_5_ = bf16[24,2048]{1,0:T(8,128)(2,1)S(1)} collective-permute-done((bf16[24,2048]{1,0:T(8,128)(2,1)}, bf16[24,2048]{1,0:T(8,128)(2,1)S(1)}, u32[]{:S(2)}, u32[]{:S(2)}) %collective-permute-start.5) | collective-permute-done | bytes 98336 | tf_op jit(solution)/shard_map/ppermute | solution.py:253
  109.1 2.1 %collective-permute-start = (bf16[2,1024]{1,0:T(2,128)(2,1)S(1)}, bf16[2,1024]{1,0:T(2,128)(2,1)S(1)}, u32[]{:S(2)}, u32[]{:S(2)}) collective-permute-start(bf16[2,1024]{1,0:T(2,128)(2,1)S(1)} %multiply_convert_fusion.1), channel_id=1, source_target_pairs={{0,1},{1,2},{2,3},{3,4},{4,5},{5,6},{6,7},{7,8},{8,9},{9,10},{10,1... | collective-permute-start | bytes 12296 | tf_op jit(solution)/shard_map/ppermute | solution.py:25
  111.9 10.6 %shard_map.132 = (bf16[24,2048]{1,0:T(8,128)(2,1)}, bf16[24,2048]{1,0:T(8,128)(2,1)}, bf16[24,2048]{1,0:T(8,128)(2,1)}, bf16[24,2048]{1,0:T(8,128)(2,1)}, bf16[2...) custom-call(f32[1,2048]{1,0:T(1,128)} %bitcast.16, ...), custom_call_target="tpu_custom_call" | custom-call | flops 4831838208 | bytes 15728640 | tf_op jit(solution)/shard_map/pallas_call | solution.py:221
  125.7 3.1 %collective-permute-start.19 = (bf16[24,2048]{1,0:T(8,128)(2,1)S(1)}, bf16[24,2048]{1,0:T(8,128)(2,1)S(1)}, u32[]{:S(2)}, u32[]{:S(2)}) collective-permute-start(bf16[24,2048]{1,0:T(8,128)(2,1)S(1)} %copy-done.29), channel_id=1, source_target_pairs={{0,4},{1,5},{2,6},{3,7},{4,0},{5,1},{6,2},{7,3},{8,12},{9,13},{10,... | collective-permute-start | bytes 294920 | tf_op jit(solution)/shard_map/ppermute | solution.py:253
  128.8 2.8 %collective-permute-start.21 = (bf16[24,2048]{1,0:T(8,128)(2,1)S(1)}, bf16[24,2048]{1,0:T(8,128)(2,1)S(1)}, u32[]{:S(2)}, u32[]{:S(2)}) collective-permute-start(bf16[24,2048]{1,0:T(8,128)(2,1)S(1)} %copy-done.25), channel_id=1, source_target_pairs={{0,6},{1,7},{2,4},{3,5},{4,2},{5,3},{6,0},{7,1},{8,14},{9,15},{10,... | collective-permute-start | bytes 294920 | tf_op jit(solution)/shard_map/ppermute | solution.py:253
  133.5 1.8 %collective-permute-start.24 = (bf16[24,2048]{1,0:T(8,128)(2,1)S(1)}, bf16[24,2048]{1,0:T(8,128)(2,1)S(1)}, u32[]{:S(2)}, u32[]{:S(2)}) collective-permute-start(bf16[24,2048]{1,0:T(8,128)(2,1)S(1)} %copy-done.18), channel_id=1, source_target_pairs={{0,9},{1,8},{2,11},{3,10},{4,13},{5,12},{6,15},{7,14},{8,1},{9,0},... | collective-permute-start | bytes 294920 | tf_op jit(solution)/shard_map/ppermute | solution.py:253
  135.3 2.8 %collective-permute-done.20.refs_5_ = bf16[24,2048]{1,0:T(8,128)(2,1)S(1)} collective-permute-done((bf16[24,2048]{1,0:T(8,128)(2,1)S(1)}, bf16[24,2048]{1,0:T(8,128)(2,1)S(1)}, u32[]{:S(2)}, u32[]{:S(2)}) %collective-permute-start.20) | collective-permute-done | bytes 98336 | tf_op jit(solution)/shard_map/ppermute | solution.py:253
  138.1 2.2 %collective-permute-start.25 = (bf16[24,2048]{1,0:T(8,128)(2,1)S(1)}, bf16[24,2048]{1,0:T(8,128)(2,1)S(1)}, u32[]{:S(2)}, u32[]{:S(2)}) collective-permute-start(bf16[24,2048]{1,0:T(8,128)(2,1)S(1)} %copy-done.15), channel_id=1, source_target_pairs={{0,10},{1,11},{2,8},{3,9},{4,14},{5,15},{6,12},{7,13},{8,2},{9,3},... | collective-permute-start | bytes 294920 | tf_op jit(solution)/shard_map/ppermute | solution.py:253
  143.1 2.0 %collective-permute-start.27 = (bf16[24,2048]{1,0:T(8,128)(2,1)S(1)}, bf16[24,2048]{1,0:T(8,128)(2,1)S(1)}, u32[]{:S(2)}, u32[]{:S(2)}) collective-permute-start(bf16[24,2048]{1,0:T(8,128)(2,1)S(1)} %copy-done.11), channel_id=1, source_target_pairs={{0,12},{1,13},{2,14},{3,15},{4,8},{5,9},{6,10},{7,11},{8,4},{9,5},... | collective-permute-start | bytes 294920 | tf_op jit(solution)/shard_map/ppermute | solution.py:253
  146.0 2.2 %collective-permute-start.29 = (bf16[24,2048]{1,0:T(8,128)(2,1)S(1)}, bf16[24,2048]{1,0:T(8,128)(2,1)S(1)}, u32[]{:S(2)}, u32[]{:S(2)}) collective-permute-start(bf16[24,2048]{1,0:T(8,128)(2,1)S(1)} %copy-done.9), channel_id=1, source_target_pairs={{0,14},{1,15},{2,12},{3,13},{4,10},{5,11},{6,8},{7,9},{8,6},{9,7},... | collective-permute-start | bytes 294920 | tf_op jit(solution)/shard_map/ppermute | solution.py:253
  150.5 8.2 %convolution_convert_fusion = bf16[512,2048]{1,0:T(8,128)(2,1)} fusion(bf16[1024,2048]{1,0:T(8,128)(2,1)} %param.16, f32[514,1024]{1,0:T(8,128)} %maximum_convert_fusion, bf16[512,1024]{1,0:T(8,128)(2,1)S(1)} %copy-done.7, f32[1024]{0:T(1024)S(1)} %bitcast.19, f32[1024]{0:T(1024)S(1)} %bitcast.20, f32[1024]{0:T(1024)S(1)} %bitcast.18), kind=kOutput, calls=%fused_computation | convolution fusion | flops 2152726528 | bytes 13643776 | tf_op jit(solution)/shard_map/dot_general | solution.py:280
  158.7 16.4 %collective-permute-done.34.refs_16_ = bf16[128,2048]{1,0:T(8,128)(2,1)S(1)} collective-permute-done((bf16[128,2048]{1,0:T(8,128)(2,1)S(1)}, bf16[128,2048]{1,0:T(8,128)(2,1)S(1)}, u32[]{:S(2)}, u32[]{:S(2)}) %collective-permute-start.34) | collective-permute-done | bytes 524320 | tf_op jit(solution)/shard_map/ppermute | solution.py:36
  (132 shorter events, 22.9 us)
Async XLA Ops:
  0.6 25.3 %collective-permute-start.32 = (bf16[128,2048]{1,0:T(8,128)(2,1)}, bf16[128,2048]{1,0:T(8,128)(2,1)S(1)}, u32[]{:S(2)}, u32[]{:S(2)}) collective-permute-start(bf16[128,2048]{1,0:T(8,128)(2,1)} %rows_ref.1), channel_id=1, source_target_pairs={{0,24},{4,28},{8,16},{12,20},{16,8},{20,12},{24,0},{28,4},{1,25},{... | collective-permute-start | bytes 1572872 | tf_op jit(solution)/shard_map/ppermute | solution.py:36
  1.2 24.7 %collective-permute-start.31 = (s32[4,128]{1,0:T(4,128)}, s32[4,128]{1,0:T(4,128)S(1)}, u32[]{:S(2)}, u32[]{:S(2)}) collective-permute-start(s32[4,128]{1,0:T(4,128)} %bitcast.21), channel_id=1, source_target_pairs={{0,24},{4,28},{8,16},{12,20},{16,8},{20,12},{24,0},{28,4},{1,25},{... | collective-permute-start | bytes 6152 | tf_op jit(solution)/shard_map/ppermute | solution.py:36
  61.2 81.1 %all-to-all-start.1 = ((bf16[16,24,2048]{2,1,0:T(8,128)(2,1)}), bf16[16,24,2048]{2,1,0:T(8,128)(2,1)S(1)}, u32[]{:S(2)}, u32[]{:S(2)}) async-start(bf16[16,24,2048]{2,1,0:T(8,128)(2,1)} %bitcast.8), calls=%async_computation.1 | async-start | bytes 3145728 | tf_op jit(solution)/shard_map/all_to_all | solution.py:265
  68.2 21.5 %collective-permute-start.10 = (bf16[24,2048]{1,0:T(8,128)(2,1)}, bf16[24,2048]{1,0:T(8,128)(2,1)S(1)}, u32[]{:S(2)}, u32[]{:S(2)}) collective-permute-start(bf16[24,2048]{1,0:T(8,128)(2,1)} %get-tuple-element.48), channel_id=1, source_target_pairs={{0,10},{1,11},{2,8},{3,9},{4,14},{5,15},{6,12},{7,13},{8,2},{9,3},... | collective-permute-start | bytes 294920 | tf_op jit(solution)/shard_map/ppermute | solution.py:253
  70.8 19.9 %collective-permute-start.11 = (bf16[24,2048]{1,0:T(8,128)(2,1)}, bf16[24,2048]{1,0:T(8,128)(2,1)S(1)}, u32[]{:S(2)}, u32[]{:S(2)}) collective-permute-start(bf16[24,2048]{1,0:T(8,128)(2,1)} %get-tuple-element.49), channel_id=1, source_target_pairs={{0,11},{1,10},{2,9},{3,8},{4,15},{5,14},{6,13},{7,12},{8,3},{9,2},... | collective-permute-start | bytes 294920 | tf_op jit(solution)/shard_map/ppermute | solution.py:253
  70.8 23.3 %collective-permute-start.12 = (bf16[24,2048]{1,0:T(8,128)(2,1)}, bf16[24,2048]{1,0:T(8,128)(2,1)S(1)}, u32[]{:S(2)}, u32[]{:S(2)}) collective-permute-start(bf16[24,2048]{1,0:T(8,128)(2,1)} %get-tuple-element.50), channel_id=1, source_target_pairs={{0,12},{1,13},{2,14},{3,15},{4,8},{5,9},{6,10},{7,11},{8,4},{9,5},... | collective-permute-start | bytes 294920 | tf_op jit(solution)/shard_map/ppermute | solution.py:253
  73.4 21.6 %collective-permute-start.13 = (bf16[24,2048]{1,0:T(8,128)(2,1)}, bf16[24,2048]{1,0:T(8,128)(2,1)S(1)}, u32[]{:S(2)}, u32[]{:S(2)}) collective-permute-start(bf16[24,2048]{1,0:T(8,128)(2,1)} %get-tuple-element.51), channel_id=1, source_target_pairs={{0,13},{1,12},{2,15},{3,14},{4,9},{5,8},{6,11},{7,10},{8,5},{9,4},... | collective-permute-start | bytes 294920 | tf_op jit(solution)/shard_map/ppermute | solution.py:253
  73.5 25.3 %collective-permute-start.14 = (bf16[24,2048]{1,0:T(8,128)(2,1)}, bf16[24,2048]{1,0:T(8,128)(2,1)S(1)}, u32[]{:S(2)}, u32[]{:S(2)}) collective-permute-start(bf16[24,2048]{1,0:T(8,128)(2,1)} %get-tuple-element.52), channel_id=1, source_target_pairs={{0,14},{1,15},{2,12},{3,13},{4,10},{5,11},{6,8},{7,9},{8,6},{9,7},... | collective-permute-start | bytes 294920 | tf_op jit(solution)/shard_map/ppermute | solution.py:253
  89.7 10.1 %collective-permute-start.15 = (bf16[24,2048]{1,0:T(8,128)(2,1)}, bf16[24,2048]{1,0:T(8,128)(2,1)S(1)}, u32[]{:S(2)}, u32[]{:S(2)}) collective-permute-start(bf16[24,2048]{1,0:T(8,128)(2,1)} %get-tuple-element.53), channel_id=1, source_target_pairs={{0,15},{1,14},{2,13},{3,12},{4,11},{5,10},{6,9},{7,8},{8,7},{9,6},... | collective-permute-start | bytes 294920 | tf_op jit(solution)/shard_map/ppermute | solution.py:253
  90.7 10.1 %collective-permute-start.2 = (bf16[24,2048]{1,0:T(8,128)(2,1)}, bf16[24,2048]{1,0:T(8,128)(2,1)S(1)}, u32[]{:S(2)}, u32[]{:S(2)}) collective-permute-start(bf16[24,2048]{1,0:T(8,128)(2,1)} %get-tuple-element.40), channel_id=1, source_target_pairs={{0,2},{1,3},{2,0},{3,1},{4,6},{5,7},{6,4},{7,5},{8,10},{9,11},{10,... | collective-permute-start | bytes 294920 | tf_op jit(solution)/shard_map/ppermute | solution.py:253
  98.7 10.0 %collective-permute-start.5 = (bf16[24,2048]{1,0:T(8,128)(2,1)}, bf16[24,2048]{1,0:T(8,128)(2,1)S(1)}, u32[]{:S(2)}, u32[]{:S(2)}) collective-permute-start(bf16[24,2048]{1,0:T(8,128)(2,1)} %get-tuple-element.43), channel_id=1, source_target_pairs={{0,5},{1,4},{2,7},{3,6},{4,1},{5,0},{6,3},{7,2},{8,13},{9,12},{10,... | collective-permute-start | bytes 294920 | tf_op jit(solution)/shard_map/ppermute | solution.py:253
  100.8 10.4 %collective-permute-start.7 = (bf16[24,2048]{1,0:T(8,128)(2,1)}, bf16[24,2048]{1,0:T(8,128)(2,1)S(1)}, u32[]{:S(2)}, u32[]{:S(2)}) collective-permute-start(bf16[24,2048]{1,0:T(8,128)(2,1)} %get-tuple-element.45), channel_id=1, source_target_pairs={{0,7},{1,6},{2,5},{3,4},{4,3},{5,2},{6,1},{7,0},{8,15},{9,14},{10,... | collective-permute-start | bytes 294920 | tf_op jit(solution)/shard_map/ppermute | solution.py:253
  108.7 17.0 %collective-permute-start.33 = (f32[4,128]{1,0:T(4,128)S(1)}, f32[4,128]{1,0:T(4,128)S(1)}, u32[]{:S(2)}, u32[]{:S(2)}) collective-permute-start(f32[4,128]{1,0:T(4,128)S(1)} %bitcast.14), channel_id=1, source_target_pairs={{0,24},{4,28},{8,16},{12,20},{16,8},{20,12},{24,0},{28,4},{1,25},{... | collective-permute-start | bytes 6152 | tf_op jit(solution)/shard_map/ppermute | solution.py:36
  109.1 19.7 %collective-permute-start = (bf16[2,1024]{1,0:T(2,128)(2,1)S(1)}, bf16[2,1024]{1,0:T(2,128)(2,1)S(1)}, u32[]{:S(2)}, u32[]{:S(2)}) collective-permute-start(bf16[2,1024]{1,0:T(2,128)(2,1)S(1)} %multiply_convert_fusion.1), channel_id=1, source_target_pairs={{0,1},{1,2},{2,3},{3,4},{4,5},{5,6},{6,7},{7,8},{8,9},{9,10},{10,1... | collective-permute-start | bytes 12296 | tf_op jit(solution)/shard_map/ppermute | solution.py:25
  128.8 11.5 %collective-permute-start.21 = (bf16[24,2048]{1,0:T(8,128)(2,1)S(1)}, bf16[24,2048]{1,0:T(8,128)(2,1)S(1)}, u32[]{:S(2)}, u32[]{:S(2)}) collective-permute-start(bf16[24,2048]{1,0:T(8,128)(2,1)S(1)} %copy-done.25), channel_id=1, source_target_pairs={{0,6},{1,7},{2,4},{3,5},{4,2},{5,3},{6,0},{7,1},{8,14},{9,15},{10,... | collective-permute-start | bytes 294920 | tf_op jit(solution)/shard_map/ppermute | solution.py:253
  131.7 11.4 %collective-permute-start.22 = (bf16[24,2048]{1,0:T(8,128)(2,1)}, bf16[24,2048]{1,0:T(8,128)(2,1)S(1)}, u32[]{:S(2)}, u32[]{:S(2)}) collective-permute-start(bf16[24,2048]{1,0:T(8,128)(2,1)} %get-tuple-element.61), channel_id=1, source_target_pairs={{0,7},{1,6},{2,5},{3,4},{4,3},{5,2},{6,1},{7,0},{8,15},{9,14},{10,... | collective-permute-start | bytes 294920 | tf_op jit(solution)/shard_map/ppermute | solution.py:253
  132.1 13.1 %collective-permute-start.23 = (bf16[24,2048]{1,0:T(8,128)(2,1)S(1)}, bf16[24,2048]{1,0:T(8,128)(2,1)S(1)}, u32[]{:S(2)}, u32[]{:S(2)}) collective-permute-start(bf16[24,2048]{1,0:T(8,128)(2,1)S(1)} %copy-done.20), channel_id=1, source_target_pairs={{0,8},{1,9},{2,10},{3,11},{4,12},{5,13},{6,14},{7,15},{8,0},{9,1},... | collective-permute-start | bytes 294920 | tf_op jit(solution)/shard_map/ppermute | solution.py:253
  133.5 12.6 %collective-permute-start.24 = (bf16[24,2048]{1,0:T(8,128)(2,1)S(1)}, bf16[24,2048]{1,0:T(8,128)(2,1)S(1)}, u32[]{:S(2)}, u32[]{:S(2)}) collective-permute-start(bf16[24,2048]{1,0:T(8,128)(2,1)S(1)} %copy-done.18), channel_id=1, source_target_pairs={{0,9},{1,8},{2,11},{3,10},{4,13},{5,12},{6,15},{7,14},{8,1},{9,0},... | collective-permute-start | bytes 294920 | tf_op jit(solution)/shard_map/ppermute | solution.py:253
  138.1 10.2 %collective-permute-start.25 = (bf16[24,2048]{1,0:T(8,128)(2,1)S(1)}, bf16[24,2048]{1,0:T(8,128)(2,1)S(1)}, u32[]{:S(2)}, u32[]{:S(2)}) collective-permute-start(bf16[24,2048]{1,0:T(8,128)(2,1)S(1)} %copy-done.15), channel_id=1, source_target_pairs={{0,10},{1,11},{2,8},{3,9},{4,14},{5,15},{6,12},{7,13},{8,2},{9,3},... | collective-permute-start | bytes 294920 | tf_op jit(solution)/shard_map/ppermute | solution.py:253
  143.1 15.5 %collective-permute-start.27 = (bf16[24,2048]{1,0:T(8,128)(2,1)S(1)}, bf16[24,2048]{1,0:T(8,128)(2,1)S(1)}, u32[]{:S(2)}, u32[]{:S(2)}) collective-permute-start(bf16[24,2048]{1,0:T(8,128)(2,1)S(1)} %copy-done.11), channel_id=1, source_target_pairs={{0,12},{1,13},{2,14},{3,15},{4,8},{5,9},{6,10},{7,11},{8,4},{9,5},... | collective-permute-start | bytes 294920 | tf_op jit(solution)/shard_map/ppermute | solution.py:253
  145.1 13.5 %collective-permute-start.28 = (bf16[24,2048]{1,0:T(8,128)(2,1)S(1)}, bf16[24,2048]{1,0:T(8,128)(2,1)S(1)}, u32[]{:S(2)}, u32[]{:S(2)}) collective-permute-start(bf16[24,2048]{1,0:T(8,128)(2,1)S(1)} %copy-done.10), channel_id=1, source_target_pairs={{0,13},{1,12},{2,15},{3,14},{4,9},{5,8},{6,11},{7,10},{8,5},{9,4},... | collective-permute-start | bytes 294920 | tf_op jit(solution)/shard_map/ppermute | solution.py:253
  146.0 12.6 %collective-permute-start.29 = (bf16[24,2048]{1,0:T(8,128)(2,1)S(1)}, bf16[24,2048]{1,0:T(8,128)(2,1)S(1)}, u32[]{:S(2)}, u32[]{:S(2)}) collective-permute-start(bf16[24,2048]{1,0:T(8,128)(2,1)S(1)} %copy-done.9), channel_id=1, source_target_pairs={{0,14},{1,15},{2,12},{3,13},{4,10},{5,11},{6,8},{7,9},{8,6},{9,7},... | collective-permute-start | bytes 294920 | tf_op jit(solution)/shard_map/ppermute | solution.py:253
  148.3 10.4 %collective-permute-start.30 = (bf16[24,2048]{1,0:T(8,128)(2,1)S(1)}, bf16[24,2048]{1,0:T(8,128)(2,1)S(1)}, u32[]{:S(2)}, u32[]{:S(2)}) collective-permute-start(bf16[24,2048]{1,0:T(8,128)(2,1)S(1)} %copy-done.8), channel_id=1, source_target_pairs={{0,15},{1,14},{2,13},{3,12},{4,11},{5,10},{6,9},{7,8},{8,7},{9,6},... | collective-permute-start | bytes 294920 | tf_op jit(solution)/shard_map/ppermute | solution.py:253
  149.4 25.7 %collective-permute-start.34 = (bf16[128,2048]{1,0:T(8,128)(2,1)S(1)}, bf16[128,2048]{1,0:T(8,128)(2,1)S(1)}, u32[]{:S(2)}, u32[]{:S(2)}) collective-permute-start(bf16[128,2048]{1,0:T(8,128)(2,1)S(1)} %shard_map.135), channel_id=1, source_target_pairs={{0,24},{4,28},{8,16},{12,20},{16,8},{20,12},{24,0},{28,4},{1,25},{... | collective-permute-start | bytes 1572872 | tf_op jit(solution)/shard_map/ppermute | solution.py:36
  (48 other events, 580.4 us)
where the time goes:
time: 177 us
  waiting for transfers between devices  69.4 us (39%)
  starting transfers between devices  43.5 us (25%)
  Pallas kernels  25.7 us (15%)
  blocking collectives  25.4 us (14%)
  matrix products  8.15 us (5%)
  other arithmetic  2.77 us (2%)
    ppermute x4, waiting for transfers between devices, swap_halves(): return lax.ppermute(value, ('half', 'near'), pairs)  39.5 us
    ppermute x30, starting transfers between devices, hops(): lax.ppermute(blocks[mask], NEAR, [(i, i ^ mask) for i in range(members)])  34 us
    ppermute x30, waiting for transfers between devices, hops(): lax.ppermute(blocks[mask], NEAR, [(i, i ^ mask) for i in range(members)])  29.8 us
    all_to_all x1, blocking collectives, exchange(): lax.all_to_all(parts, NEAR, split_axis=0, concat_axis=0, tiled=True)  25.4 us
    pallas_call x2, Pallas kernels, expert_rows(): pl.pallas_call(functools.partial(expert_kernel, len(rows)), in_specs=[pl....  19.8 us
    dot_general x1, matrix products, mixer(): jnp.dot(gated_rows, mixer_out_weight, preferred_element_type=jnp.float32)  8.15 us
    all_to_all x1, starting transfers between devices, exchange(): lax.all_to_all(parts, NEAR, split_axis=0, concat_axis=0, tiled=True)  3.85 us
    ppermute x4, starting transfers between devices, swap_halves(): return lax.ppermute(value, ('half', 'near'), pairs)  3.55 us
  transfers between devices with their start and end apart: 36, of which 12 were waited for; matrix products, arithmetic and copies ran while one was open for 6% of the time, Pallas kernels for 8%

commit v1 on v0

--- a/solution.py
+++ b/solution.py
@@ -152,7 +152,10 @@
 
 def expert_kernel(blocks, gain, gate, up, down, *refs):
     in_refs, out_refs = refs[:blocks], refs[blocks : 2 * blocks]
-    gate_ref, up_ref, down_ref, hidden_ref, wide_ref, rows_ref, gain_ref, sems = refs[2 * blocks :]
+    gate_ref, up_ref, down_ref, hidden_ref, wide_ref, rows_ref, gain_ref, sems = refs[
+        2 * blocks : 2 * blocks + 8
+    ]
+    leaving = []
     parts, _, tile = gate_ref.shape
     columns, _, column = down_ref.shape
     work = []
@@ -182,13 +185,14 @@
         for copy in copies[step]:
             copy.start()
     height = in_refs[0].shape[0]
-    for block, ref in enumerate(in_refs):
+    for block, ref in enumerate(in_refs if blocks > 1 else ()):
         wide_ref[block * height : (block + 1) * height, :] = ref[...].astype(jnp.float32)
     scale_copy.wait()
     count = wide_ref.shape[0]
     band = math.gcd(count, 64)
     for top in range(0, count, band):
-        tokens = wide_ref[top : top + band, :]
+        source = wide_ref if blocks > 1 else in_refs[0]
+        tokens = source[top : top + band, :].astype(jnp.float32)
         scale = lax.rsqrt(jnp.mean(tokens * tokens, axis=-1, keepdims=True) + epsilon)
         rows_ref[top : top + band, :] = (tokens * scale * gain_ref[...]).astype(jnp.bfloat16)
     for part in range(parts):
@@ -204,12 +208,23 @@
     for part in range(columns):
         ready(parts + part)
         result = jnp.dot(hidden_ref[...], down_ref[part], preferred_element_type=jnp.float32)
+        cut = slice(part * column, (part + 1) * column)
+        if blocks == 1:
+            made_ref = refs[-1]
+            made_ref[part] = result.astype(made_ref.dtype)
+            leaving.append(
+                pltpu.make_async_copy(
+                    made_ref.at[part], out_refs[0].at[:, cut], sems.at[len(copies) + 1 + part, 0]
+                )
+            )
+            leaving[-1].start()
+            continue
         start = 0
         for ref in out_refs:
-            ref[:, part * column : (part + 1) * column] = result[
-                start : start + ref.shape[0]
-            ].astype(ref.dtype)
+            ref[:, cut] = result[start : start + ref.shape[0]].astype(ref.dtype)
             start += ref.shape[0]
+    for copy in leaving:
+        copy.wait()
 
 
 def expert_rows(rows, gain, weights, room):
@@ -221,7 +236,7 @@
     return pl.pallas_call(
         functools.partial(expert_kernel, len(rows)),
         in_specs=[pl.BlockSpec(memory_space=pl.ANY)] * 4 + [held] * len(rows),
-        out_specs=[held] * len(rows),
+        out_specs=[pl.BlockSpec(memory_space=pl.ANY) if len(rows) == 1 else held] * len(rows),
         out_shape=block_shapes(count, width, len(rows)),
         scratch_shapes=[
             pltpu.VMEM((parts, width, tile), jnp.bfloat16),
@@ -231,7 +246,8 @@
             pltpu.VMEM((count, width), jnp.float32),
             pltpu.VMEM((count, width), jnp.bfloat16),
             pltpu.VMEM(gain.shape, gain.dtype),
-            pltpu.SemaphoreType.DMA((parts + columns + 1, 2)),
+            pltpu.SemaphoreType.DMA((parts + 2 * columns + 1, 2)),
+            pltpu.VMEM((columns, count, column), jnp.bfloat16),
         ],
         compiler_params=pltpu.CompilerParams(vmem_limit_bytes=room),
         cost_estimate=pl.CostEstimate(

time: 177 us -> 177 us (level)
  no operation moved by 1% of the time
where the time goes in v1:
time: 177 us; the launch traced here: 176 us
  waiting for transfers between devices  69.4 us (39%)
  starting transfers between devices  43.5 us (25%)
  Pallas kernels  25.5 us (14%)
  blocking collectives  25.4 us (14%)
  matrix products  8.15 us (5%)
  other arithmetic  2.77 us (2%)
    ppermute x4, waiting for transfers between devices, swap_halves(): return lax.ppermute(value, ('half', 'near'), pairs)  39.6 us
    ppermute x30, starting transfers between devices, hops(): lax.ppermute(blocks[mask], NEAR, [(i, i ^ mask) for i in range(members)])  34 us
    ppermute x30, waiting for transfers between devices, hops(): lax.ppermute(blocks[mask], NEAR, [(i, i ^ mask) for i in range(members)])  29.8 us
    all_to_all x1, blocking collectives, exchange(): lax.all_to_all(parts, NEAR, split_axis=0, concat_axis=0, tiled=True)  25.4 us
    pallas_call x2, Pallas kernels, expert_rows(): pl.pallas_call(functools.partial(expert_kernel, len(rows)), in_specs=[pl....  19.5 us
    dot_general x1, matrix products, mixer(): jnp.dot(gated_rows, mixer_out_weight, preferred_element_type=jnp.float32)  8.15 us
    all_to_all x1, starting transfers between devices, exchange(): lax.all_to_all(parts, NEAR, split_axis=0, concat_axis=0, tiled=True)  3.85 us
  transfers between devices with their start and end apart: 36, of which 12 were waited for; matrix products, arithmetic and copies ran while one was open for 6% of the time, Pallas kernels for 8%

profile of v1, /device:TPU:16, one launch (start us, length us, event | category | flops | bytes accessed | tf_op | source)
XLA Modules:
  0.0 176.4 jit_solution(13519219478437429025)
XLA Ops:
  2.7 23.2 %collective-permute-done.31.ids_ref = s32[4,128]{1,0:T(4,128)S(1)} collective-permute-done((s32[4,128]{1,0:T(4,128)}, s32[4,128]{1,0:T(4,128)S(1)}, u32[]{:S(2)}, u32[]{:S(2)}) %collective-permute-start.31) | collective-permute-done | bytes 2080 | tf_op jit(solution)/shard_map/ppermute | solution.py:36
  26.6 25.4 %all_to_all.10 = bf16[16,24,2048]{2,1,0:T(8,128)(2,1)S(1)} all-to-all(bf16[16,24,2048]{2,1,0:T(8,128)(2,1)S(1)} %bitcast.12), channel_id=1, replica_groups=mesh['half'=2,'near'=4,'tp'=4] {'near','tp'}, dimensions={0} | all-to-all | bytes 3145728 | tf_op jit(solution)/shard_map/all_to_all | solution.py:281
  52.0 8.8 %shard_map.134 = bf16[384,2048]{1,0:T(8,128)(2,1)} custom-call(f32[1,2048]{1,0:T(1,128)S(1)} %bitcast.17, bf16[1,2048,1024]{2,1,0:T(8,128)(2,1)} %gate.3, bf16[1,2048,1024]{2,1,0:T(8,128)(2,1)} %up.3, bf16[1,1024,2048]{2,1,0:T(8,128)(2,1)} %down.3, bf16[384,2048]{1,0:T(8,128)(2,1)S(1)} %bitcast.13), custom_call_target="tpu_custom_call" | custom-call | flops 4831838208 | bytes 15728640 | tf_op jit(solution)/shard_map/pallas_call | solution.py:236
  60.9 3.9 %all-to-all-start.1 = ((bf16[16,24,2048]{2,1,0:T(8,128)(2,1)}), bf16[16,24,2048]{2,1,0:T(8,128)(2,1)S(1)}, u32[]{:S(2)}, u32[]{:S(2)}) async-start(bf16[16,24,2048]{2,1,0:T(8,128)(2,1)} %bitcast.8), calls=%async_computation.1 | async-start | bytes 3145728 | tf_op jit(solution)/shard_map/all_to_all | solution.py:281
  64.7 2.8 %shard_map.131 = (s32[4,128]{1,0:T(4,128)}, bf16[24,2048]{1,0:T(8,128)(2,1)}, bf16[24,2048]{1,0:T(8,128)(2,1)}, bf16[24,2048]{1,0:T(8,128)(2,1)}, bf16[24,2048]{...) custom-call(s32[4,128]{1,0:T(4,128)} %bitcast.22, ...), custom_call_target="tpu_custom_call" | custom-call | flops 201326592 | bytes 2097152 | tf_op jit(solution)/shard_map/pallas_call | solution.py:86
  67.8 2.6 %collective-permute-start.10 = (bf16[24,2048]{1,0:T(8,128)(2,1)}, bf16[24,2048]{1,0:T(8,128)(2,1)S(1)}, u32[]{:S(2)}, u32[]{:S(2)}) collective-permute-start(bf16[24,2048]{1,0:T(8,128)(2,1)} %get-tuple-element.48), channel_id=1, source_target_pairs={{0,10},{1,11},{2,8},{3,9},{4,14},{5,15},{6,12},{7,13},{8,2},{9,3},... | collective-permute-start | bytes 294920 | tf_op jit(solution)/shard_map/ppermute | solution.py:269
  70.4 2.7 %collective-permute-start.12 = (bf16[24,2048]{1,0:T(8,128)(2,1)}, bf16[24,2048]{1,0:T(8,128)(2,1)S(1)}, u32[]{:S(2)}, u32[]{:S(2)}) collective-permute-start(bf16[24,2048]{1,0:T(8,128)(2,1)} %get-tuple-element.50), channel_id=1, source_target_pairs={{0,12},{1,13},{2,14},{3,15},{4,8},{5,9},{6,10},{7,11},{8,4},{9,5},... | collective-permute-start | bytes 294920 | tf_op jit(solution)/shard_map/ppermute | solution.py:269
  73.1 3.5 %collective-permute-start.14 = (bf16[24,2048]{1,0:T(8,128)(2,1)}, bf16[24,2048]{1,0:T(8,128)(2,1)S(1)}, u32[]{:S(2)}, u32[]{:S(2)}) collective-permute-start(bf16[24,2048]{1,0:T(8,128)(2,1)} %get-tuple-element.52), channel_id=1, source_target_pairs={{0,14},{1,15},{2,12},{3,13},{4,10},{5,11},{6,8},{7,9},{8,6},{9,7},... | collective-permute-start | bytes 294920 | tf_op jit(solution)/shard_map/ppermute | solution.py:269
  76.6 12.7 %collective-permute-done.10.refs_10_ = bf16[24,2048]{1,0:T(8,128)(2,1)S(1)} collective-permute-done((bf16[24,2048]{1,0:T(8,128)(2,1)}, bf16[24,2048]{1,0:T(8,128)(2,1)S(1)}, u32[]{:S(2)}, u32[]{:S(2)}) %collective-permute-start.10) | collective-permute-done | bytes 98336 | tf_op jit(solution)/shard_map/ppermute | solution.py:269
  90.4 3.3 %collective-permute-done.12.refs_12_ = bf16[24,2048]{1,0:T(8,128)(2,1)S(1)} collective-permute-done((bf16[24,2048]{1,0:T(8,128)(2,1)}, bf16[24,2048]{1,0:T(8,128)(2,1)S(1)}, u32[]{:S(2)}, u32[]{:S(2)}) %collective-permute-start.12) | collective-permute-done | bytes 98336 | tf_op jit(solution)/shard_map/ppermute | solution.py:269
  94.7 3.7 %collective-permute-done.14.refs_14_ = bf16[24,2048]{1,0:T(8,128)(2,1)S(1)} collective-permute-done((bf16[24,2048]{1,0:T(8,128)(2,1)}, bf16[24,2048]{1,0:T(8,128)(2,1)S(1)}, u32[]{:S(2)}, u32[]{:S(2)}) %collective-permute-start.14) | collective-permute-done | bytes 98336 | tf_op jit(solution)/shard_map/ppermute | solution.py:269
  100.4 1.7 collective-permute-start.7
  104.7 3.7 %collective-permute-done.5.refs_5_ = bf16[24,2048]{1,0:T(8,128)(2,1)S(1)} collective-permute-done((bf16[24,2048]{1,0:T(8,128)(2,1)}, bf16[24,2048]{1,0:T(8,128)(2,1)S(1)}, u32[]{:S(2)}, u32[]{:S(2)}) %collective-permute-start.5) | collective-permute-done | bytes 98336 | tf_op jit(solution)/shard_map/ppermute | solution.py:269
  108.8 2.1 %collective-permute-start = (bf16[2,1024]{1,0:T(2,128)(2,1)S(1)}, bf16[2,1024]{1,0:T(2,128)(2,1)S(1)}, u32[]{:S(2)}, u32[]{:S(2)}) collective-permute-start(bf16[2,1024]{1,0:T(2,128)(2,1)S(1)} %multiply_convert_fusion.1), channel_id=1, source_target_pairs={{0,1},{1,2},{2,3},{3,4},{4,5},{5,6},{6,7},{7,8},{8,9},{9,10},{10,1... | collective-permute-start | bytes 12296 | tf_op jit(solution)/shard_map/ppermute | solution.py:25
  111.6 10.7 %shard_map.132 = (bf16[24,2048]{1,0:T(8,128)(2,1)}, bf16[24,2048]{1,0:T(8,128)(2,1)}, bf16[24,2048]{1,0:T(8,128)(2,1)}, bf16[24,2048]{1,0:T(8,128)(2,1)}, bf16[2...) custom-call(f32[1,2048]{1,0:T(1,128)} %bitcast.16, ...), custom_call_target="tpu_custom_call" | custom-call | flops 4831838208 | bytes 15728640 | tf_op jit(solution)/shard_map/pallas_call | solution.py:236
  125.4 3.1 %collective-permute-start.19 = (bf16[24,2048]{1,0:T(8,128)(2,1)S(1)}, bf16[24,2048]{1,0:T(8,128)(2,1)S(1)}, u32[]{:S(2)}, u32[]{:S(2)}) collective-permute-start(bf16[24,2048]{1,0:T(8,128)(2,1)S(1)} %copy-done.29), channel_id=1, source_target_pairs={{0,4},{1,5},{2,6},{3,7},{4,0},{5,1},{6,2},{7,3},{8,12},{9,13},{10,... | collective-permute-start | bytes 294920 | tf_op jit(solution)/shard_map/ppermute | solution.py:269
  128.6 2.8 %collective-permute-start.21 = (bf16[24,2048]{1,0:T(8,128)(2,1)S(1)}, bf16[24,2048]{1,0:T(8,128)(2,1)S(1)}, u32[]{:S(2)}, u32[]{:S(2)}) collective-permute-start(bf16[24,2048]{1,0:T(8,128)(2,1)S(1)} %copy-done.25), channel_id=1, source_target_pairs={{0,6},{1,7},{2,4},{3,5},{4,2},{5,3},{6,0},{7,1},{8,14},{9,15},{10,... | collective-permute-start | bytes 294920 | tf_op jit(solution)/shard_map/ppermute | solution.py:269
  133.2 1.9 %collective-permute-start.24 = (bf16[24,2048]{1,0:T(8,128)(2,1)S(1)}, bf16[24,2048]{1,0:T(8,128)(2,1)S(1)}, u32[]{:S(2)}, u32[]{:S(2)}) collective-permute-start(bf16[24,2048]{1,0:T(8,128)(2,1)S(1)} %copy-done.18), channel_id=1, source_target_pairs={{0,9},{1,8},{2,11},{3,10},{4,13},{5,12},{6,15},{7,14},{8,1},{9,0},... | collective-permute-start | bytes 294920 | tf_op jit(solution)/shard_map/ppermute | solution.py:269
  135.1 2.8 %collective-permute-done.20.refs_5_ = bf16[24,2048]{1,0:T(8,128)(2,1)S(1)} collective-permute-done((bf16[24,2048]{1,0:T(8,128)(2,1)S(1)}, bf16[24,2048]{1,0:T(8,128)(2,1)S(1)}, u32[]{:S(2)}, u32[]{:S(2)}) %collective-permute-start.20) | collective-permute-done | bytes 98336 | tf_op jit(solution)/shard_map/ppermute | solution.py:269
  137.9 2.2 %collective-permute-start.25 = (bf16[24,2048]{1,0:T(8,128)(2,1)S(1)}, bf16[24,2048]{1,0:T(8,128)(2,1)S(1)}, u32[]{:S(2)}, u32[]{:S(2)}) collective-permute-start(bf16[24,2048]{1,0:T(8,128)(2,1)S(1)} %copy-done.15), channel_id=1, source_target_pairs={{0,10},{1,11},{2,8},{3,9},{4,14},{5,15},{6,12},{7,13},{8,2},{9,3},... | collective-permute-start | bytes 294920 | tf_op jit(solution)/shard_map/ppermute | solution.py:269
  142.9 2.0 %collective-permute-start.27 = (bf16[24,2048]{1,0:T(8,128)(2,1)S(1)}, bf16[24,2048]{1,0:T(8,128)(2,1)S(1)}, u32[]{:S(2)}, u32[]{:S(2)}) collective-permute-start(bf16[24,2048]{1,0:T(8,128)(2,1)S(1)} %copy-done.11), channel_id=1, source_target_pairs={{0,12},{1,13},{2,14},{3,15},{4,8},{5,9},{6,10},{7,11},{8,4},{9,5},... | collective-permute-start | bytes 294920 | tf_op jit(solution)/shard_map/ppermute | solution.py:269
  145.8 2.2 %collective-permute-start.29 = (bf16[24,2048]{1,0:T(8,128)(2,1)S(1)}, bf16[24,2048]{1,0:T(8,128)(2,1)S(1)}, u32[]{:S(2)}, u32[]{:S(2)}) collective-permute-start(bf16[24,2048]{1,0:T(8,128)(2,1)S(1)} %copy-done.9), channel_id=1, source_target_pairs={{0,14},{1,15},{2,12},{3,13},{4,10},{5,11},{6,8},{7,9},{8,6},{9,7},... | collective-permute-start | bytes 294920 | tf_op jit(solution)/shard_map/ppermute | solution.py:269
  150.2 8.2 %convolution_convert_fusion = bf16[512,2048]{1,0:T(8,128)(2,1)} fusion(bf16[1024,2048]{1,0:T(8,128)(2,1)} %param.16, f32[514,1024]{1,0:T(8,128)} %maximum_convert_fusion, bf16[512,1024]{1,0:T(8,128)(2,1)S(1)} %copy-done.7, f32[1024]{0:T(1024)S(1)} %bitcast.19, f32[1024]{0:T(1024)S(1)} %bitcast.20, f32[1024]{0:T(1024)S(1)} %bitcast.18), kind=kOutput, calls=%fused_computation | convolution fusion | flops 2152726528 | bytes 13643776 | tf_op jit(solution)/shard_map/dot_general | solution.py:296
  158.4 16.4 %collective-permute-done.34.refs_16_ = bf16[128,2048]{1,0:T(8,128)(2,1)S(1)} collective-permute-done((bf16[128,2048]{1,0:T(8,128)(2,1)S(1)}, bf16[128,2048]{1,0:T(8,128)(2,1)S(1)}, u32[]{:S(2)}, u32[]{:S(2)}) %collective-permute-start.34) | collective-permute-done | bytes 524320 | tf_op jit(solution)/shard_map/ppermute | solution.py:36
  (132 shorter events, 22.9 us)
Async XLA Ops:
  0.6 25.3 %collective-permute-start.32 = (bf16[128,2048]{1,0:T(8,128)(2,1)}, bf16[128,2048]{1,0:T(8,128)(2,1)S(1)}, u32[]{:S(2)}, u32[]{:S(2)}) collective-permute-start(bf16[128,2048]{1,0:T(8,128)(2,1)} %rows_ref.1), channel_id=1, source_target_pairs={{0,24},{4,28},{8,16},{12,20},{16,8},{20,12},{24,0},{28,4},{1,25},{... | collective-permute-start | bytes 1572872 | tf_op jit(solution)/shard_map/ppermute | solution.py:36
  1.2 24.7 %collective-permute-start.31 = (s32[4,128]{1,0:T(4,128)}, s32[4,128]{1,0:T(4,128)S(1)}, u32[]{:S(2)}, u32[]{:S(2)}) collective-permute-start(s32[4,128]{1,0:T(4,128)} %bitcast.21), channel_id=1, source_target_pairs={{0,24},{4,28},{8,16},{12,20},{16,8},{20,12},{24,0},{28,4},{1,25},{... | collective-permute-start | bytes 6152 | tf_op jit(solution)/shard_map/ppermute | solution.py:36
  60.9 81.2 %all-to-all-start.1 = ((bf16[16,24,2048]{2,1,0:T(8,128)(2,1)}), bf16[16,24,2048]{2,1,0:T(8,128)(2,1)S(1)}, u32[]{:S(2)}, u32[]{:S(2)}) async-start(bf16[16,24,2048]{2,1,0:T(8,128)(2,1)} %bitcast.8), calls=%async_computation.1 | async-start | bytes 3145728 | tf_op jit(solution)/shard_map/all_to_all | solution.py:281
  67.8 21.5 %collective-permute-start.10 = (bf16[24,2048]{1,0:T(8,128)(2,1)}, bf16[24,2048]{1,0:T(8,128)(2,1)S(1)}, u32[]{:S(2)}, u32[]{:S(2)}) collective-permute-start(bf16[24,2048]{1,0:T(8,128)(2,1)} %get-tuple-element.48), channel_id=1, source_target_pairs={{0,10},{1,11},{2,8},{3,9},{4,14},{5,15},{6,12},{7,13},{8,2},{9,3},... | collective-permute-start | bytes 294920 | tf_op jit(solution)/shard_map/ppermute | solution.py:269
  70.4 19.9 %collective-permute-start.11 = (bf16[24,2048]{1,0:T(8,128)(2,1)}, bf16[24,2048]{1,0:T(8,128)(2,1)S(1)}, u32[]{:S(2)}, u32[]{:S(2)}) collective-permute-start(bf16[24,2048]{1,0:T(8,128)(2,1)} %get-tuple-element.49), channel_id=1, source_target_pairs={{0,11},{1,10},{2,9},{3,8},{4,15},{5,14},{6,13},{7,12},{8,3},{9,2},... | collective-permute-start | bytes 294920 | tf_op jit(solution)/shard_map/ppermute | solution.py:269
  70.4 23.3 %collective-permute-start.12 = (bf16[24,2048]{1,0:T(8,128)(2,1)}, bf16[24,2048]{1,0:T(8,128)(2,1)S(1)}, u32[]{:S(2)}, u32[]{:S(2)}) collective-permute-start(bf16[24,2048]{1,0:T(8,128)(2,1)} %get-tuple-element.50), channel_id=1, source_target_pairs={{0,12},{1,13},{2,14},{3,15},{4,8},{5,9},{6,10},{7,11},{8,4},{9,5},... | collective-permute-start | bytes 294920 | tf_op jit(solution)/shard_map/ppermute | solution.py:269
  73.1 21.6 %collective-permute-start.13 = (bf16[24,2048]{1,0:T(8,128)(2,1)}, bf16[24,2048]{1,0:T(8,128)(2,1)S(1)}, u32[]{:S(2)}, u32[]{:S(2)}) collective-permute-start(bf16[24,2048]{1,0:T(8,128)(2,1)} %get-tuple-element.51), channel_id=1, source_target_pairs={{0,13},{1,12},{2,15},{3,14},{4,9},{5,8},{6,11},{7,10},{8,5},{9,4},... | collective-permute-start | bytes 294920 | tf_op jit(solution)/shard_map/ppermute | solution.py:269
  73.1 25.3 %collective-permute-start.14 = (bf16[24,2048]{1,0:T(8,128)(2,1)}, bf16[24,2048]{1,0:T(8,128)(2,1)S(1)}, u32[]{:S(2)}, u32[]{:S(2)}) collective-permute-start(bf16[24,2048]{1,0:T(8,128)(2,1)} %get-tuple-element.52), channel_id=1, source_target_pairs={{0,14},{1,15},{2,12},{3,13},{4,10},{5,11},{6,8},{7,9},{8,6},{9,7},... | collective-permute-start | bytes 294920 | tf_op jit(solution)/shard_map/ppermute | solution.py:269
  89.4 10.1 %collective-permute-start.15 = (bf16[24,2048]{1,0:T(8,128)(2,1)}, bf16[24,2048]{1,0:T(8,128)(2,1)S(1)}, u32[]{:S(2)}, u32[]{:S(2)}) collective-permute-start(bf16[24,2048]{1,0:T(8,128)(2,1)} %get-tuple-element.53), channel_id=1, source_target_pairs={{0,15},{1,14},{2,13},{3,12},{4,11},{5,10},{6,9},{7,8},{8,7},{9,6},... | collective-permute-start | bytes 294920 | tf_op jit(solution)/shard_map/ppermute | solution.py:269
  90.3 10.1 %collective-permute-start.2 = (bf16[24,2048]{1,0:T(8,128)(2,1)}, bf16[24,2048]{1,0:T(8,128)(2,1)S(1)}, u32[]{:S(2)}, u32[]{:S(2)}) collective-permute-start(bf16[24,2048]{1,0:T(8,128)(2,1)} %get-tuple-element.40), channel_id=1, source_target_pairs={{0,2},{1,3},{2,0},{3,1},{4,6},{5,7},{6,4},{7,5},{8,10},{9,11},{10,... | collective-permute-start | bytes 294920 | tf_op jit(solution)/shard_map/ppermute | solution.py:269
  98.4 10.0 %collective-permute-start.5 = (bf16[24,2048]{1,0:T(8,128)(2,1)}, bf16[24,2048]{1,0:T(8,128)(2,1)S(1)}, u32[]{:S(2)}, u32[]{:S(2)}) collective-permute-start(bf16[24,2048]{1,0:T(8,128)(2,1)} %get-tuple-element.43), channel_id=1, source_target_pairs={{0,5},{1,4},{2,7},{3,6},{4,1},{5,0},{6,3},{7,2},{8,13},{9,12},{10,... | collective-permute-start | bytes 294920 | tf_op jit(solution)/shard_map/ppermute | solution.py:269
  100.4 10.5 %collective-permute-start.7 = (bf16[24,2048]{1,0:T(8,128)(2,1)}, bf16[24,2048]{1,0:T(8,128)(2,1)S(1)}, u32[]{:S(2)}, u32[]{:S(2)}) collective-permute-start(bf16[24,2048]{1,0:T(8,128)(2,1)} %get-tuple-element.45), channel_id=1, source_target_pairs={{0,7},{1,6},{2,5},{3,4},{4,3},{5,2},{6,1},{7,0},{8,15},{9,14},{10,... | collective-permute-start | bytes 294920 | tf_op jit(solution)/shard_map/ppermute | solution.py:269
  108.4 17.0 %collective-permute-start.33 = (f32[4,128]{1,0:T(4,128)S(1)}, f32[4,128]{1,0:T(4,128)S(1)}, u32[]{:S(2)}, u32[]{:S(2)}) collective-permute-start(f32[4,128]{1,0:T(4,128)S(1)} %bitcast.14), channel_id=1, source_target_pairs={{0,24},{4,28},{8,16},{12,20},{16,8},{20,12},{24,0},{28,4},{1,25},{... | collective-permute-start | bytes 6152 | tf_op jit(solution)/shard_map/ppermute | solution.py:36
  108.8 19.8 %collective-permute-start = (bf16[2,1024]{1,0:T(2,128)(2,1)S(1)}, bf16[2,1024]{1,0:T(2,128)(2,1)S(1)}, u32[]{:S(2)}, u32[]{:S(2)}) collective-permute-start(bf16[2,1024]{1,0:T(2,128)(2,1)S(1)} %multiply_convert_fusion.1), channel_id=1, source_target_pairs={{0,1},{1,2},{2,3},{3,4},{4,5},{5,6},{6,7},{7,8},{8,9},{9,10},{10,1... | collective-permute-start | bytes 12296 | tf_op jit(solution)/shard_map/ppermute | solution.py:25
  128.6 11.5 %collective-permute-start.21 = (bf16[24,2048]{1,0:T(8,128)(2,1)S(1)}, bf16[24,2048]{1,0:T(8,128)(2,1)S(1)}, u32[]{:S(2)}, u32[]{:S(2)}) collective-permute-start(bf16[24,2048]{1,0:T(8,128)(2,1)S(1)} %copy-done.25), channel_id=1, source_target_pairs={{0,6},{1,7},{2,4},{3,5},{4,2},{5,3},{6,0},{7,1},{8,14},{9,15},{10,... | collective-permute-start | bytes 294920 | tf_op jit(solution)/shard_map/ppermute | solution.py:269
  131.4 11.4 %collective-permute-start.22 = (bf16[24,2048]{1,0:T(8,128)(2,1)}, bf16[24,2048]{1,0:T(8,128)(2,1)S(1)}, u32[]{:S(2)}, u32[]{:S(2)}) collective-permute-start(bf16[24,2048]{1,0:T(8,128)(2,1)} %get-tuple-element.61), channel_id=1, source_target_pairs={{0,7},{1,6},{2,5},{3,4},{4,3},{5,2},{6,1},{7,0},{8,15},{9,14},{10,... | collective-permute-start | bytes 294920 | tf_op jit(solution)/shard_map/ppermute | solution.py:269
  131.8 13.1 %collective-permute-start.23 = (bf16[24,2048]{1,0:T(8,128)(2,1)S(1)}, bf16[24,2048]{1,0:T(8,128)(2,1)S(1)}, u32[]{:S(2)}, u32[]{:S(2)}) collective-permute-start(bf16[24,2048]{1,0:T(8,128)(2,1)S(1)} %copy-done.20), channel_id=1, source_target_pairs={{0,8},{1,9},{2,10},{3,11},{4,12},{5,13},{6,14},{7,15},{8,0},{9,1},... | collective-permute-start | bytes 294920 | tf_op jit(solution)/shard_map/ppermute | solution.py:269
  133.2 12.6 %collective-permute-start.24 = (bf16[24,2048]{1,0:T(8,128)(2,1)S(1)}, bf16[24,2048]{1,0:T(8,128)(2,1)S(1)}, u32[]{:S(2)}, u32[]{:S(2)}) collective-permute-start(bf16[24,2048]{1,0:T(8,128)(2,1)S(1)} %copy-done.18), channel_id=1, source_target_pairs={{0,9},{1,8},{2,11},{3,10},{4,13},{5,12},{6,15},{7,14},{8,1},{9,0},... | collective-permute-start | bytes 294920 | tf_op jit(solution)/shard_map/ppermute | solution.py:269
  137.9 10.1 %collective-permute-start.25 = (bf16[24,2048]{1,0:T(8,128)(2,1)S(1)}, bf16[24,2048]{1,0:T(8,128)(2,1)S(1)}, u32[]{:S(2)}, u32[]{:S(2)}) collective-permute-start(bf16[24,2048]{1,0:T(8,128)(2,1)S(1)} %copy-done.15), channel_id=1, source_target_pairs={{0,10},{1,11},{2,8},{3,9},{4,14},{5,15},{6,12},{7,13},{8,2},{9,3},... | collective-permute-start | bytes 294920 | tf_op jit(solution)/shard_map/ppermute | solution.py:269
  142.9 15.5 %collective-permute-start.27 = (bf16[24,2048]{1,0:T(8,128)(2,1)S(1)}, bf16[24,2048]{1,0:T(8,128)(2,1)S(1)}, u32[]{:S(2)}, u32[]{:S(2)}) collective-permute-start(bf16[24,2048]{1,0:T(8,128)(2,1)S(1)} %copy-done.11), channel_id=1, source_target_pairs={{0,12},{1,13},{2,14},{3,15},{4,8},{5,9},{6,10},{7,11},{8,4},{9,5},... | collective-permute-start | bytes 294920 | tf_op jit(solution)/shard_map/ppermute | solution.py:269
  144.9 13.5 %collective-permute-start.28 = (bf16[24,2048]{1,0:T(8,128)(2,1)S(1)}, bf16[24,2048]{1,0:T(8,128)(2,1)S(1)}, u32[]{:S(2)}, u32[]{:S(2)}) collective-permute-start(bf16[24,2048]{1,0:T(8,128)(2,1)S(1)} %copy-done.10), channel_id=1, source_target_pairs={{0,13},{1,12},{2,15},{3,14},{4,9},{5,8},{6,11},{7,10},{8,5},{9,4},... | collective-permute-start | bytes 294920 | tf_op jit(solution)/shard_map/ppermute | solution.py:269
  145.8 12.6 %collective-permute-start.29 = (bf16[24,2048]{1,0:T(8,128)(2,1)S(1)}, bf16[24,2048]{1,0:T(8,128)(2,1)S(1)}, u32[]{:S(2)}, u32[]{:S(2)}) collective-permute-start(bf16[24,2048]{1,0:T(8,128)(2,1)S(1)} %copy-done.9), channel_id=1, source_target_pairs={{0,14},{1,15},{2,12},{3,13},{4,10},{5,11},{6,8},{7,9},{8,6},{9,7},... | collective-permute-start | bytes 294920 | tf_op jit(solution)/shard_map/ppermute | solution.py:269
  148.0 10.4 %collective-permute-start.30 = (bf16[24,2048]{1,0:T(8,128)(2,1)S(1)}, bf16[24,2048]{1,0:T(8,128)(2,1)S(1)}, u32[]{:S(2)}, u32[]{:S(2)}) collective-permute-start(bf16[24,2048]{1,0:T(8,128)(2,1)S(1)} %copy-done.8), channel_id=1, source_target_pairs={{0,15},{1,14},{2,13},{3,12},{4,11},{5,10},{6,9},{7,8},{8,7},{9,6},... | collective-permute-start | bytes 294920 | tf_op jit(solution)/shard_map/ppermute | solution.py:269
  149.2 25.7 %collective-permute-start.34 = (bf16[128,2048]{1,0:T(8,128)(2,1)S(1)}, bf16[128,2048]{1,0:T(8,128)(2,1)S(1)}, u32[]{:S(2)}, u32[]{:S(2)}) collective-permute-start(bf16[128,2048]{1,0:T(8,128)(2,1)S(1)} %shard_map.135), channel_id=1, source_target_pairs={{0,24},{4,28},{8,16},{12,20},{16,8},{20,12},{24,0},{28,4},{1,25},{... | collective-permute-start | bytes 1572872 | tf_op jit(solution)/shard_map/ppermute | solution.py:36
  (48 other events, 580.9 us)
